TPU v7x, 32 devices: a whole 2x2x4 slice. The times are simulated.
32 devices in a mesh: rep: 8 (over z, y), fs: 2 (over x), tp: 2 (over core).
Axes of the slice: x: 2, y: 2, z: 4, core: 2. Of those that a mesh axis runs over, the one named last changes fastest.
Arguments:
- inputs: bfloat16 [4096, 2048], P(('rep', 'tp'), 'fs'), may hold values from -6 to 6
- pre_act: bfloat16 [4096, 4096], P(('rep', 'fs'), 'tp'), may hold values from -6 to 6
- cotangent: bfloat16 [4096, 2048], P(('rep', 'tp'), 'fs'), may hold values from -6 to 6
- up_weight: bfloat16 [2048, 4096], P('fs', 'tp'), may hold values from -0.125 to 0.125
- down_weight: bfloat16 [4096, 2048], P('tp', 'fs'), may hold values from -0.09375 to 0.09375
Outputs:
- grad_inputs: bfloat16 [4096, 2048], P(('rep', 'tp'), 'fs')
- grad_up: float32 [2048, 4096], P('fs', 'tp')
- grad_down: float32 [4096, 2048], P('tp', 'fs')
All inputs are finite; a program needn't handle non-finite values.
Results may differ from a plain program's by a relative error of at most 0.015.
Values may be sent and summed in bfloat16 or wider, within the bound.
A program may use at most 128 MiB of HBM per device.

v0:
```python
import jax
import jax.numpy as jnp
from jax import lax
from jax.sharding import PartitionSpec as P


def contract_rows(left, right):
    return lax.dot_general(
        left, right, (((0,), (0,)), ((), ())), preferred_element_type=jnp.float32
    )


def contract_cols(left, right):
    return lax.dot_general(
        left, right, (((1,), (1,)), ((), ())), preferred_element_type=jnp.float32
    )


def per_device(inputs, pre_act, cotangent, up_weight, down_weight):
    group_x, group_cot = (
        lax.all_gather(inputs, "tp", axis=0, tiled=True),
        lax.all_gather(cotangent, "tp", axis=0, tiled=True),
    )
    positive = jnp.maximum(pre_act.astype(jnp.float32), 0.0)
    square = (positive * positive).astype(jnp.bfloat16)
    rows_block = group_cot
    grad_act = lax.psum_scatter(
        contract_cols(rows_block, down_weight).astype(jnp.bfloat16),
        "fs",
        scatter_dimension=0,
        tiled=True,
    ).astype(jnp.float32)
    grad_pre = (2.0 * positive * grad_act).astype(jnp.bfloat16)
    factor = (inputs.shape[0] * lax.axis_size("rep") * lax.axis_size("tp")) ** (-0.5)
    group_grad, group_square = (
        lax.all_gather(grad_pre, "fs", axis=0, tiled=True),
        lax.all_gather(square, "fs", axis=0, tiled=True),
    )
    down_part = contract_rows(group_square, group_cot)
    up_part = contract_rows(group_x, group_grad)
    up_slice, down_slice = (
        lax.psum_scatter(up_part, "rep", scatter_dimension=0, tiled=True),
        lax.psum_scatter(down_part, "rep", scatter_dimension=0, tiled=True),
    )
    grad_up, grad_down = (
        lax.all_gather(up_slice.astype(jnp.bfloat16), "rep", axis=0, tiled=True).astype(
            up_slice.dtype
        ),
        lax.all_gather(down_slice.astype(jnp.bfloat16), "rep", axis=0, tiled=True).astype(
            down_slice.dtype
        ),
    )
    rows_block = group_grad
    grad_inputs = lax.psum_scatter(
        contract_cols(rows_block, up_weight).astype(jnp.bfloat16),
        "tp",
        scatter_dimension=0,
        tiled=True,
    )
    return (grad_inputs, grad_up * factor, grad_down * factor)


def solution(mesh):
    placed = (
        P(("rep", "tp"), "fs"),
        P(("rep", "fs"), "tp"),
        P(("rep", "tp"), "fs"),
        P("fs", "tp"),
        P("tp", "fs"),
    )
    return jax.shard_map(
        per_device,
        mesh=mesh,
        in_specs=placed,
        out_specs=(P(("rep", "tp"), "fs"), P("fs", "tp"), P("tp", "fs")),
        check_vma=False,
    )
```

profile of v0, /device:TPU:0, one launch (start us, length us, event | category | flops | bytes accessed | tf_op | source)
XLA Modules:
  0.0 611.5 jit_solution(11408372984345961125)
XLA Ops:
  7.2 0.7 all-gather.7.cloned.1.call-update
  7.9 0.0 reduce-scatter.5.cloned.1.call-start
  8.0 13.3 %all-gather.7.cloned.1.call-done = bf16[512,1024]{1,0:T(8,128)(2,1)} async-done(((bf16[256,1024]{1,0:T(8,128)(2,1)}), bf16[512,1024]{1,0:T(8,128)(2,1)}) %all-gather.7.cloned.1.call-update) | async-done | bytes 1048592 | tf_op jit(solution)/shard_map/all_gather | solution.py:22
  21.3 6.2 %convolution_convert_fusion = bf16[512,2048]{1,0:T(8,128)(2,1)} fusion(bf16[512,1024]{1,0:T(8,128)(2,1)} %all-gather.7.cloned.1.call-done, bf16[2048,1024]{1,0:T(8,128)(2,1)} %param.9), kind=kOutput, calls=%fused_computation.3 | convolution fusion | flops 2148532224 | bytes 7340032 | tf_op jit(solution)/shard_map/dot_general | solution.py:14
  27.5 0.0 all-gather.11.cloned.1.call-start
  27.6 0.7 all-gather.11.cloned.1.call-update
  28.3 0.0 all-gather.9.cloned.1.call-start
  28.3 32.5 %reduce-scatter.5.cloned.1.call-done = bf16[256,2048]{1,0:T(8,128)(2,1)} async-done(((bf16[512,2048]{1,0:T(8,128)(2,1)}), bf16[256,2048]{1,0:T(8,128)(2,1)}) %reduce-scatter.5.cloned.1.call-update) | async-done | bytes 1048592 | tf_op jit(solution)/shard_map/reduce_scatter | solution.py:27
  60.8 3.1 multiply_convert_fusion
  63.9 0.0 all-gather.15.cloned.1.call-start
  64.0 0.5 all-gather.15.cloned.1.call-update
  64.5 0.0 reduce-scatter.9.cloned.1.call-start
  64.5 6.8 %all-gather.11.cloned.1.call-done = bf16[512,1024]{1,0:T(8,128)(2,1)} async-done(((bf16[256,1024]{1,0:T(8,128)(2,1)}), bf16[512,1024]{1,0:T(8,128)(2,1)}) %all-gather.11.cloned.1.call-update) | async-done | bytes 1048592 | tf_op jit(solution)/shard_map/all_gather | solution.py:21
  71.4 36.3 %all-gather.9.cloned.1.call-done = bf16[512,2048]{1,0:T(8,128)(2,1)} async-done(((bf16[256,2048]{1,0:T(8,128)(2,1)}), bf16[512,2048]{1,0:T(8,128)(2,1)}) %all-gather.9.cloned.1.call-update) | async-done | bytes 2097168 | tf_op jit(solution)/shard_map/all_gather | solution.py:36
  107.7 7.6 %convolution_bitcast_fusion = f32[1024,2048]{0,1:T(8,128)} fusion(bf16[512,2048]{1,0:T(8,128)(2,1)} %all-gather.9.cloned.1.call-done, bf16[512,1024]{1,0:T(8,128)(2,1)} %all-gather.11.cloned.1.call-done), kind=kOutput, calls=%fused_computation.2 | convolution fusion | flops 2147483648 | bytes 11534336 | tf_op jit(solution)/shard_map/dot_general | solution.py:8
  115.3 0.0 reduce-scatter.11.cloned.1.call-start
  115.4 27.4 %all-gather.15.cloned.1.call-done = bf16[512,2048]{1,0:T(8,128)(2,1)} async-done(((bf16[256,2048]{1,0:T(8,128)(2,1)}), bf16[512,2048]{1,0:T(8,128)(2,1)}) %all-gather.15.cloned.1.call-update) | async-done | bytes 2097168 | tf_op jit(solution)/shard_map/all_gather | solution.py:37
  142.7 7.4 %fusion = f32[2048,1024]{1,0:T(8,128)} fusion(bf16[512,2048]{1,0:T(8,128)(2,1)} %all-gather.15.cloned.1.call-done, bf16[512,1024]{1,0:T(8,128)(2,1)S(1)} %copy-done.2), kind=kOutput, calls=%fused_computation.8 | convolution fusion | flops 2147483648 | bytes 11534336 | tf_op jit(solution)/shard_map/dot_general | solution.py:8
  150.1 0.0 all-gather.13.cloned.1.call-start
  150.2 144.5 %reduce-scatter.9.cloned.1.call-done = f32[128,2048]{0,1:T(8,128)} async-done(((f32[1024,2048]{0,1:T(8,128)}), f32[128,2048]{0,1:T(8,128)}) %reduce-scatter.9.cloned.1.call-update) | async-done | bytes 1048592 | tf_op jit(solution)/shard_map/reduce_scatter | solution.py:42
  294.7 2.1 convert_element_type.35
  296.8 0.0 all-gather.17.cloned.1.call-start
  296.8 148.7 %reduce-scatter.11.cloned.1.call-done = f32[256,1024]{1,0:T(8,128)} async-done(((f32[2048,1024]{1,0:T(8,128)}), f32[256,1024]{1,0:T(8,128)}) %reduce-scatter.11.cloned.1.call-update) | async-done | bytes 1048592 | tf_op jit(solution)/shard_map/reduce_scatter | solution.py:43
  445.5 2.1 convert_element_type.38
  447.6 0.2 reduce-scatter.7.cloned.1.call-start
  447.9 5.6 convolution_convert_fusion.1
  453.5 68.4 %all-gather.13.cloned.1.call-done = bf16[1024,2048]{0,1:T(8,128)(2,1)} async-done(((bf16[128,2048]{0,1:T(8,128)(2,1)}), bf16[1024,2048]{0,1:T(8,128)(2,1)}) %all-gather.13.cloned.1.call-update) | async-done | bytes 4194320 | tf_op jit(solution)/shard_map/all_gather | solution.py:46
  521.9 6.8 %convert_multiply_fusion.1 = f32[1024,2048]{0,1:T(8,128)} fusion(bf16[1024,2048]{0,1:T(8,128)(2,1)} %all-gather.13.cloned.1.call-done), kind=kLoop, calls=%fused_computation.1 | loop fusion | flops 4194304 | bytes 12582912 | tf_op jit(solution)/shard_map/mul | solution.py:60
  528.7 9.3 %copy.8 = f32[1024,2048]{1,0:T(8,128)} copy(f32[1024,2048]{0,1:T(8,128)} %convert_multiply_fusion.1) | data formatting | bytes 16777216
  538.0 57.1 %all-gather.17.cloned.1.call-done = bf16[2048,1024]{1,0:T(8,128)(2,1)} async-done(((bf16[256,1024]{1,0:T(8,128)(2,1)}), bf16[2048,1024]{1,0:T(8,128)(2,1)}) %all-gather.17.cloned.1.call-update) | async-done | bytes 4194320 | tf_op jit(solution)/shard_map/all_gather | solution.py:49
  595.0 6.8 %convert_multiply_fusion = f32[2048,1024]{1,0:T(8,128)} fusion(bf16[2048,1024]{1,0:T(8,128)(2,1)} %all-gather.17.cloned.1.call-done), kind=kLoop, calls=%fused_computation | loop fusion | flops 4194304 | bytes 12582912 | tf_op jit(solution)/shard_map/mul | solution.py:60
  601.8 2.8 reduce-scatter.7.cloned.1.call-done
  (14 shorter events, 0.2 us)
Async XLA Ops:
  7.2 14.1 %all-gather.7.cloned.1.call-start = ((), (), s32[]{:S(2)}) async-start(), calls=%async_computation.4 | async-start | bytes 1572864 | tf_op jit(solution)/shard_map/all_gather | solution.py:22
  7.9 52.9 %copy-start = (bf16[256,2048]{1,0:T(8,128)(2,1)S(1)}, bf16[256,2048]{1,0:T(8,128)(2,1)}, u32[]{:S(2)}) copy-start(bf16[256,2048]{1,0:T(8,128)(2,1)} %param.6) | copy-start | bytes 3145732
  7.9 52.9 %reduce-scatter.5.cloned.1.call-start = ((), (), s32[]{:S(2)}) async-start(), calls=%async_computation.5 | async-start | bytes 3145728 | tf_op jit(solution)/shard_map/reduce_scatter | solution.py:27
  27.5 43.9 %all-gather.11.cloned.1.call-start = ((), (), s32[]{:S(2)}) async-start(), calls=%async_computation.8 | async-start | bytes 1572864 | tf_op jit(solution)/shard_map/all_gather | solution.py:21
  28.3 79.4 %all-gather.9.cloned.1.call-start = ((), (), s32[]{:S(2)}) async-start(), calls=%async_computation.6 | async-start | bytes 3145728 | tf_op jit(solution)/shard_map/all_gather | solution.py:36
  63.9 78.8 %all-gather.15.cloned.1.call-start = ((), (), s32[]{:S(2)}) async-start(), calls=%async_computation.11 | async-start | bytes 3145728 | tf_op jit(solution)/shard_map/all_gather | solution.py:37
  64.5 230.2 %reduce-scatter.9.cloned.1.call-start = ((), (), s32[]{:S(2)}) async-start(), calls=%async_computation.9 | async-start | bytes 9437184 | tf_op jit(solution)/shard_map/reduce_scatter | solution.py:42
  115.3 27.5 %copy-start.2 = (bf16[512,1024]{1,0:T(8,128)(2,1)S(1)}, bf16[512,1024]{1,0:T(8,128)(2,1)}, u32[]{:S(2)}) copy-start(bf16[512,1024]{1,0:T(8,128)(2,1)} %all-gather.7.cloned.1.call-done) | copy-start | bytes 3145732
  115.3 330.2 %reduce-scatter.11.cloned.1.call-start = ((), (), s32[]{:S(2)}) async-start(), calls=%async_computation.12 | async-start | bytes 9437184 | tf_op jit(solution)/shard_map/reduce_scatter | solution.py:43
  150.1 297.7 %copy-start.1 = (bf16[512,2048]{1,0:T(8,128)(2,1)S(1)}, bf16[512,2048]{1,0:T(8,128)(2,1)}, u32[]{:S(2)}) copy-start(bf16[512,2048]{1,0:T(8,128)(2,1)} %all-gather.9.cloned.1.call-done) | copy-start | bytes 6291460
  150.1 371.7 %all-gather.13.cloned.1.call-start = ((), (), s32[]{:S(2)}) async-start(), calls=%async_computation.10 | async-start | bytes 4718592 | tf_op jit(solution)/shard_map/all_gather | solution.py:46
  296.8 298.2 %all-gather.17.cloned.1.call-start = ((), (), s32[]{:S(2)}) async-start(), calls=%async_computation.13 | async-start | bytes 4718592 | tf_op jit(solution)/shard_map/all_gather | solution.py:49
  447.6 157.0 %reduce-scatter.7.cloned.1.call-start = ((), (), s32[]{:S(2)}) async-start(), calls=%async_computation.7 | async-start | bytes 1572864 | tf_op jit(solution)/shard_map/reduce_scatter | solution.py:54
Sparse Core Ops, SparseCore 0:
  9.5 11.7 all-gather.6
  27.6 33.0 reduce-scatter.4
  62.3 9.0 all-gather.10
  73.4 34.2 all-gather.8
  109.6 33.0 all-gather.14
  146.8 147.8 reduce-scatter.8
  298.9 146.5 reduce-scatter.10
  448.1 73.7 all-gather.12
  524.0 70.9 all-gather.16
  597.7 6.8 reduce-scatter.6
where the time goes:
time: 612 us; the launch traced here: 611 us
  waiting for transfers between devices  540 us (88%)
  matrix products  26.8 us (4%)
  other arithmetic  20.9 us (3%)
  between operations  14.2 us (2%)
  local copies, waits for them, and re-layouts  9.29 us (2%)
    reduce_scatter x1, waiting for transfers between devices, per_device(): lax.psum_scatter(down_part, 'rep', scatter_dimension=0, tiled=True)  149 us
    reduce_scatter x1, waiting for transfers between devices, per_device(): lax.psum_scatter(up_part, 'rep', scatter_dimension=0, tiled=True)  144 us
    all_gather x1, waiting for transfers between devices, per_device(): lax.all_gather(up_slice.astype(jnp.bfloat16), 'rep', axis=0, tiled=True)  68.4 us
    all_gather x1, waiting for transfers between devices, per_device(): lax.all_gather(down_slice.astype(jnp.bfloat16), 'rep', axis=0, tiled=True)  57.1 us
    all_gather x1, waiting for transfers between devices, per_device(): lax.all_gather(grad_pre, 'fs', axis=0, tiled=True)  36.3 us
    reduce_scatter x1, waiting for transfers between devices, per_device(): lax.psum_scatter(contract_cols(rows_block, down_weight).astype(jnp.bfloat...  32.5 us
    all_gather x1, waiting for transfers between devices, per_device(): lax.all_gather(square, 'fs', axis=0, tiled=True)  27.4 us
    dot_general x2, matrix products, contract_rows(): lax.dot_general(left, right, (((0,), (0,)), ((), ())), preferred_element_...  15 us
  transfers between devices with their start and end apart: 10, of which 10 were waited for; matrix products, arithmetic and copies ran while one was open for 8% of the time, Pallas kernels for 0%

commit v1 on v0

v1 whole, which is shorter than its diff:
```python
import functools

import jax
import jax.numpy as jnp
from jax import lax
from jax.experimental import pallas as pl
from jax.experimental.pallas import tpu as pltpu
from jax.sharding import PartitionSpec as P

MESH = pl.DeviceIdType.MESH
LANES = 128
F32, BF16 = jnp.float32, jnp.bfloat16


def rows_dot(left, right):
    return lax.dot_general(left, right, (((0,), (0,)), ((), ())), preferred_element_type=F32)


def cols_dot(left, right):
    return lax.dot_general(left, right, (((1,), (1,)), ((), ())), preferred_element_type=F32)


def plan(n_rep, width, hidden):
    panels = hidden // LANES
    subs = 2 if width * panels // (4 * n_rep) >= 2 * LANES else 1
    per_panel = 2 * n_rep * subs // panels
    return subs, per_panel, width // per_panel


def kernel(
    n_rep, x_ref, pre_ref, cot_ref, wu_hbm, wd_hbm,
    gi_ref, up_ref, down_ref,
    wu, wd, xg, cg, pre_in, sq, gp, pa_own, pa_out, pa_in, gi_out, gi_in,
    first_d, first_u, rs_d, rs_u,
    w_sem, tp_s, tp_r, pre_s, pre_r, gp_s, gp_r, pa_s, pa_r, gi_s, gi_r,
    rsd_s, rsd_r, rsu_s, rsu_r, agd_s, agd_r, agu_s, agu_r,
):
    half, width = x_ref.shape
    hidden = pre_ref.shape[1]
    panels = hidden // LANES
    subs, per_panel, w = plan(n_rep, width, hidden)
    fine = 2 * n_rep == panels
    rep, fs, tp = lax.axis_index("rep"), lax.axis_index("fs"), lax.axis_index("tp")
    line = n_rep // 2
    row, col = rep // 2, rep % 2
    pos = jnp.where(col == 0, row, n_rep - 1 - row)

    def rep_at(p):
        p = lax.rem(p + n_rep, n_rep)
        return jnp.where(p < line, 2 * p, 2 * (n_rep - 1 - p) + 1)

    nxt, prv = rep_at(pos + 1), rep_at(pos + n_rep - 1)
    goal = ({"rep": nxt}, {"rep": prv})
    other_fs, other_tp = {"fs": 1 - fs}, {"tp": 1 - tp}
    mine_f = pl.ds(pl.multiple_of(fs * half, half), half)
    his_f = pl.ds(pl.multiple_of((1 - fs) * half, half), half)
    mine_t = pl.ds(pl.multiple_of(tp * half, half), half)
    his_t = pl.ds(pl.multiple_of((1 - tp) * half, half), half)

    def remote(src, dst, s, r, dev):
        return pltpu.make_async_remote_copy(
            src_ref=src, dst_ref=dst, send_sem=s, recv_sem=r, device_id=dev,
            device_id_type=MESH)

    load_wd = pltpu.make_async_copy(wd_hbm, wd, w_sem.at[0])
    load_wu = pltpu.make_async_copy(wu_hbm, wu, w_sem.at[1])
    load_wd.start()
    load_wu.start()

    barrier = pltpu.get_barrier_semaphore()
    for dev in (goal[0], goal[1], other_fs, other_tp):
        pl.semaphore_signal(barrier, inc=1, device_id=dev, device_id_type=MESH)
    pl.semaphore_wait(barrier, 4)

    def chunk_of(d, j):
        return lax.rem(pos + (-1 - j if d == 0 else 1 + j) + 2 * n_rep, n_rep)

    def lanes(panel):
        return pl.ds(pl.multiple_of(panel * LANES, LANES), LANES)

    def panel_of(d, j):
        return d * n_rep + chunk_of(d, j)

    def pre_copy(panel):
        return remote(pre_ref.at[:, lanes(panel)], pre_in.at[:, lanes(panel)],
                      pre_s.at[panel], pre_r.at[panel], other_fs)

    def gp_copy(panel):
        return remote(gp.at[mine_f, lanes(panel)], gp.at[mine_f, lanes(panel)],
                      gp_s.at[panel], gp_r.at[panel], other_fs)

    def in_order(body):
        if fine:
            def step(j, _):
                body(panel_of(0, j))
                body(panel_of(1, j))
                return 0
            lax.fori_loop(0, n_rep, step, 0)
        else:
            def step(j, _):
                body(j)
                return 0
            lax.fori_loop(0, panels, step, 0)

    cot_move = remote(cot_ref, cg.at[mine_t, :], tp_s.at[0], tp_r.at[0], other_tp)
    x_move = remote(x_ref, xg.at[mine_t, :], tp_s.at[1], tp_r.at[1], other_tp)
    cot_move.start()
    in_order(lambda panel: pre_copy(panel).start())
    x_move.start()
    cg[mine_t, :] = cot_ref[...]
    xg[mine_t, :] = x_ref[...]

    def square_of(block):
        positive = jnp.maximum(block.astype(F32), 0.0)
        return (positive * positive).astype(BF16)

    def own_square(j, _):
        sq[mine_f, lanes(j)] = square_of(pre_ref[:, lanes(j)])
        return 0
    lax.fori_loop(0, panels, own_square, 0)

    def pre_arrived(panel):
        pre_copy(panel).wait_recv()
        sq[his_f, lanes(panel)] = square_of(pre_in[:, lanes(panel)])

    def gp_arrived(panel):
        gp_copy(panel).wait_recv()

    def prepare(body, j):
        if fine:
            body(panel_of(0, j))
            body(panel_of(1, j))

    def where(d, chunk, sub):
        block = (d * n_rep + chunk) * subs + sub
        return lanes(block // per_panel), pl.ds(
            pl.multiple_of(lax.rem(block, per_panel) * w, w), w)

    def down_at(d, chunk, sub):
        hid, wid = where(d, chunk, sub)
        return down_ref.at[hid, wid]

    def up_at(d, chunk, sub):
        hid, wid = where(d, chunk, sub)
        return up_ref.at[wid, hid]

    def down_block(d, chunk, sub):
        hid, wid = where(d, chunk, sub)
        return rows_dot(sq[:, hid], cg[:, wid])

    def up_block(d, chunk, sub):
        hid, wid = where(d, chunk, sub)
        return rows_dot(xg[:, wid], gp[:, hid])

    def rs_copy(first, slots, s_sem, r_sem, d, sub, s, src=None):
        src = slots.at[d, sub, s - 1] if src is None else src
        return remote(src, slots.at[d, sub, s], s_sem.at[d, sub, s], r_sem.at[d, sub, s],
                      goal[d])

    def ag_copy(at, s_sem, r_sem, d, sub, s):
        chunk = lax.rem(pos + (-s if d == 0 else s) + n_rep, n_rep)
        return remote(at(d, chunk, sub), at(d, chunk, sub), s_sem.at[d, sub, s],
                      r_sem.at[d, sub, s], goal[d])

    streams = [(d, sub) for sub in range(subs) for d in range(2)]

    def rs_open(block, first, slots, s_sem, r_sem):
        for d, sub in streams:
            first[d, sub] = block(d, chunk_of(d, 0), sub).astype(BF16)
            rs_copy(first, slots, s_sem, r_sem, d, sub, 0, first.at[d, sub]).start()

    def rs_step(block, first, slots, s_sem, r_sem, j, d, sub):
        part = block(d, chunk_of(d, j), sub)
        rs_copy(first, slots, s_sem, r_sem, d, sub, j - 1, first.at[d, sub]).wait_recv()
        slots[d, sub, j - 1] = (slots[d, sub, j - 1].astype(F32) + part).astype(BF16)
        rs_copy(first, slots, s_sem, r_sem, d, sub, j).start()

    def rs_close(block, at, first, slots, s_sem, r_sem, as_, ar, d, sub):
        part = block(d, pos, sub)
        last = n_rep - 2
        rs_copy(first, slots, s_sem, r_sem, d, sub, last, first.at[d, sub]).wait_recv()
        at(d, pos, sub)[...] = (slots[d, sub, last].astype(F32) + part).astype(BF16)
        ag_copy(at, as_, ar, d, sub, 0).start()

    def ag_step(at, as_, ar, s, d, sub):
        chunk = lax.rem(pos + (-s if d == 0 else s) + n_rep, n_rep)
        remote(at(d, chunk, sub), at(d, chunk, sub), as_.at[d, sub, s - 1],
               ar.at[d, sub, s - 1], goal[d]).wait_recv()
        ag_copy(at, as_, ar, d, sub, s).start()

    def ag_close(at, as_, ar, d, sub):
        s = n_rep - 1
        chunk = lax.rem(pos + (-s if d == 0 else s) + n_rep, n_rep)
        remote(at(d, chunk, sub), at(d, chunk, sub), as_.at[d, sub, s - 1],
               ar.at[d, sub, s - 1], goal[d]).wait_recv()

    down = (first_d, rs_d, rsd_s, rsd_r)
    up = (first_u, rs_u, rsu_s, rsu_r)

    cot_move.wait_recv()
    if fine:
        prepare(pre_arrived, 0)
    else:
        in_order(pre_arrived)
    rs_open(down_block, *down)

    load_wd.wait()
    piece = min(2 * LANES, hidden)

    def act_step(n, _):
        at = pl.ds(pl.multiple_of(n * piece, piece), piece)
        pa_out[:, at] = cols_dot(cg[his_f, :], wd[at, :]).astype(BF16)
        return 0
    lax.fori_loop(0, hidden // piece, act_step, 0)
    pa_move = remote(pa_out, pa_in, pa_s, pa_r, other_fs)
    pa_move.start()

    def act_own(n, _):
        at = pl.ds(pl.multiple_of(n * piece, piece), piece)
        pa_own[:, at] = cols_dot(cg[mine_f, :], wd[at, :])
        return 0
    lax.fori_loop(0, hidden // piece, act_own, 0)

    def down_step(j, _):
        prepare(pre_arrived, j)
        for d, sub in streams:
            rs_step(down_block, *down, j, d, sub)
        return 0
    lax.fori_loop(1, n_rep - 1, down_step, 0)
    prepare(pre_arrived, n_rep - 1)
    for d, sub in streams:
        rs_close(down_block, down_at, *down, agd_s, agd_r, d, sub)

    pa_move.wait_recv()

    def pre_grad(panel):
        at = lanes(panel)
        positive = jnp.maximum(pre_ref[:, at].astype(F32), 0.0)
        grad = pa_own[:, at] + pa_in[:, at].astype(F32)
        gp[mine_f, at] = (2.0 * positive * grad).astype(BF16)
        gp_copy(panel).start()
    in_order(pre_grad)
    x_move.wait_recv()
    if fine:
        prepare(gp_arrived, 0)
    else:
        in_order(gp_arrived)
    rs_open(up_block, *up)

    def both_step(j, _):
        prepare(gp_arrived, j)
        for d, sub in streams:
            ag_step(down_at, agd_s, agd_r, j, d, sub)
            rs_step(up_block, *up, j, d, sub)
        return 0
    lax.fori_loop(1, n_rep - 1, both_step, 0)
    prepare(gp_arrived, n_rep - 1)
    for d, sub in streams:
        ag_close(down_at, agd_s, agd_r, d, sub)
        rs_close(up_block, up_at, *up, agu_s, agu_r, d, sub)

    load_wu.wait()
    wide = min(2 * LANES, width)

    def input_out(n, _):
        at = pl.ds(pl.multiple_of(n * wide, wide), wide)
        gi_out[:, at] = cols_dot(gp[his_t, :], wu[at, :]).astype(BF16)
        return 0
    lax.fori_loop(0, width // wide, input_out, 0)
    gi_move = remote(gi_out, gi_in, gi_s, gi_r, other_tp)
    gi_move.start()

    def gather_step(j, _):
        for d, sub in streams:
            ag_step(up_at, agu_s, agu_r, j, d, sub)
        return 0
    lax.fori_loop(1, n_rep - 1, gather_step, 0)

    gi_move.wait_recv()

    def input_own(n, _):
        at = pl.ds(pl.multiple_of(n * wide, wide), wide)
        own = cols_dot(gp[mine_t, :], wu[at, :]).astype(BF16).astype(F32)
        gi_ref[:, at] = (own + gi_in[:, at].astype(F32)).astype(BF16)
        return 0
    lax.fori_loop(0, width // wide, input_own, 0)
    for d, sub in streams:
        ag_close(up_at, agu_s, agu_r, d, sub)

    for move in (cot_move, x_move, pa_move, gi_move):
        move.wait_send()

    def sent_panels(j, _):
        pre_copy(j).wait_send()
        gp_copy(j).wait_send()
        return 0
    lax.fori_loop(0, panels, sent_panels, 0)

    def sent_steps(s, _):
        for d, sub in streams:
            rs_copy(*down, d, sub, s, first_d.at[d, sub]).wait_send()
            rs_copy(*up, d, sub, s, first_u.at[d, sub]).wait_send()
            ag_copy(down_at, agd_s, agd_r, d, sub, s).wait_send()
            ag_copy(up_at, agu_s, agu_r, d, sub, s).wait_send()
        return 0
    lax.fori_loop(0, n_rep - 1, sent_steps, 0)


def per_device(n_rep, inputs, pre_act, cotangent, up_weight, down_weight):
    half, width = inputs.shape
    hidden = pre_act.shape[1]
    panels = hidden // LANES
    subs, per_panel, w = plan(n_rep, width, hidden)
    dma = pltpu.SemaphoreType.DMA
    ring = [dma((2, subs, n_rep - 1))] * 2
    vmem = pl.BlockSpec(memory_space=pltpu.VMEM)
    anywhere = pl.BlockSpec(memory_space=pl.ANY)
    grad_inputs, grad_up, grad_down = pl.pallas_call(
        functools.partial(kernel, n_rep),
        name="ffn_backward",
        out_shape=(
            jax.ShapeDtypeStruct((half, width), BF16),
            jax.ShapeDtypeStruct((width, hidden), BF16),
            jax.ShapeDtypeStruct((hidden, width), BF16),
        ),
        in_specs=[vmem, vmem, vmem, anywhere, anywhere],
        out_specs=(vmem, vmem, vmem),
        scratch_shapes=[
            pltpu.VMEM((width, hidden), BF16),
            pltpu.VMEM((hidden, width), BF16),
            pltpu.VMEM((2 * half, width), BF16),
            pltpu.VMEM((2 * half, width), BF16),
            pltpu.VMEM((half, hidden), BF16),
            pltpu.VMEM((2 * half, hidden), BF16),
            pltpu.VMEM((2 * half, hidden), BF16),
            pltpu.VMEM((half, hidden), F32),
            pltpu.VMEM((half, hidden), BF16),
            pltpu.VMEM((half, hidden), BF16),
            pltpu.VMEM((half, width), BF16),
            pltpu.VMEM((half, width), BF16),
            pltpu.VMEM((2, subs, LANES, w), BF16),
            pltpu.VMEM((2, subs, w, LANES), BF16),
            pltpu.VMEM((2, subs, n_rep - 1, LANES, w), BF16),
            pltpu.VMEM((2, subs, n_rep - 1, w, LANES), BF16),
            dma((2,)), dma((2,)), dma((2,)),
            dma((panels,)), dma((panels,)), dma((panels,)), dma((panels,)),
            dma, dma, dma, dma,
            *ring, *ring, *ring, *ring,
        ],
        compiler_params=pltpu.CompilerParams(
            collective_id=0, has_side_effects=True, vmem_limit_bytes=58 * 2**20
        ),
    )(inputs, pre_act, cotangent, up_weight, down_weight)
    factor = (half * n_rep * lax.axis_size("tp")) ** (-0.5)
    return grad_inputs, grad_up.astype(F32) * factor, grad_down.astype(F32) * factor


def solution(mesh):
    assert mesh.shape["fs"] == 2 and mesh.shape["tp"] == 2
    placed = (
        P(("rep", "tp"), "fs"),
        P(("rep", "fs"), "tp"),
        P(("rep", "tp"), "fs"),
        P("fs", "tp"),
        P("tp", "fs"),
    )
    return jax.shard_map(
        functools.partial(per_device, mesh.shape["rep"]),
        mesh=mesh,
        in_specs=placed,
        out_specs=(P(("rep", "tp"), "fs"), P("fs", "tp"), P("tp", "fs")),
        check_vma=False,
    )
```

time: 612 us -> 193 us (0.32)
  waiting for transfers between devices: 540 us -> 0 us
  Pallas kernels: 0 us -> 180 us
  matrix products: 26.8 us -> 0 us
  between operations: 14.2 us -> 0.65 us
  other arithmetic: 20.9 us -> 11.5 us
  local copies, waits for them, and re-layouts: 9.29 us -> 0.8 us
    reduce_scatter x4 -> x0, waiting for transfers between devices: 328 us -> none  [the longest x1 149 us: per_device(): lax.psum_scatter(down_part, 'rep', scatter_dimension=0, tiled=True)]
    all_gather x6 -> x0, waiting for transfers between devices: 209 us -> none  [the longest x1 68.4 us: per_device(): lax.all_gather(up_slice.astype(jnp.bfloat16), 'rep', axis=0, tiled=True)]
    pallas_call x0 -> x1, Pallas kernels: none -> 180 us  [per_device(): pl.pallas_call(functools.partial(kernel, n_rep), name='ffn_backward', out...]
    dot_general x4 -> x0, matrix products: 26.8 us -> none  [the longest x2 15 us: contract_rows(): lax.dot_general(left, right, (((0,), (0,)), ((), ())), preferred_element_...]
    unnamed x7 -> x5, local copies, waits for them, and re-layouts: 9.29 us -> 0.8 us
    convert_element_type x3 -> x0, other arithmetic: 7.29 us -> none  [the longest x1 3.12 us: per_device(): square = (positive * positive).astype(jnp.bfloat16)]
  transfers between devices with their start and end apart: 10 -> 0, of which waited for: 10 -> 0; matrix products, arithmetic and copies ran while one was open for 8% -> 0% of each run, Pallas kernels for 0% -> 0%
where the time goes in v1:
time: 193 us
  Pallas kernels  180 us (93%)
  other arithmetic  11.5 us (6%)
    pallas_call x1, Pallas kernels, per_device(): pl.pallas_call(functools.partial(kernel, n_rep), name='ffn_backward', out...  180 us
    mul x1, other arithmetic, per_device(): grad_up.astype(F32) * factor  6.93 us
    mul x1, other arithmetic, per_device(): grad_down.astype(F32) * factor  4.59 us

profile of v1, /device:TPU:0, one launch (start us, length us, event | category | flops | bytes accessed | tf_op | source)
XLA Modules:
  0.0 192.6 jit_solution(17437192009000959438)
XLA Ops:
  0.6 179.6 %ffn_backward.1 = (bf16[256,1024]{1,0:T(8,128)(2,1)}, bf16[1024,2048]{1,0:T(8,128)(2,1)}, bf16[2048,1024]{1,0:T(8,128)(2,1)}) custom-call(bf16[256,1024]{1,0:T(8,128)(2,1)} %x_ref.1, bf16[256,2048]{1,0:T(8,128)(2,1)} %pre_ref.1, bf16[256,1024]{1,0:T(8,128)(2,1)} %cot_ref.1, bf16[1024,2048]{1,0:T(8,128)(2,1)} %wu_hbm.1, bf16[2048,1024]{1,0:T(8,128)(2,1)} %wd_hbm.1), custom_call_target="tpu_custom_call" | custom-call | tf_op jit(solution)/shard_map/ffn_backward/pallas_call | solution.py:318
  180.3 0.0 copy-start
  180.3 6.9 %convert_multiply_fusion.1 = f32[1024,2048]{1,0:T(8,128)} fusion(bf16[1024,2048]{1,0:T(8,128)(2,1)} %get-tuple-element.7), kind=kLoop, calls=%fused_computation.1 | loop fusion | flops 4194304 | bytes 12582912 | tf_op jit(solution)/shard_map/mul | solution.py:355
  187.2 0.0 copy-done
  187.2 0.0 copy-start.1
  187.2 4.6 %convert_multiply_fusion = f32[2048,1024]{1,0:T(8,128)} fusion(bf16[2048,1024]{1,0:T(8,128)(2,1)S(1)} %copy-done), kind=kLoop, calls=%fused_computation | loop fusion | flops 4194304 | bytes 12582912 | tf_op jit(solution)/shard_map/mul | solution.py:355
  191.8 0.0 copy-done.1
  191.8 0.8 copy.9
Async XLA Ops:
  180.3 6.9 %copy-start = (bf16[2048,1024]{1,0:T(8,128)(2,1)S(1)}, bf16[2048,1024]{1,0:T(8,128)(2,1)}, u32[]{:S(2)}) copy-start(bf16[2048,1024]{1,0:T(8,128)(2,1)} %get-tuple-element.8) | copy-start | bytes 12582916
  187.2 4.6 %copy-start.1 = (bf16[256,1024]{1,0:T(8,128)(2,1)S(1)}, bf16[256,1024]{1,0:T(8,128)(2,1)}, u32[]{:S(2)}) copy-start(bf16[256,1024]{1,0:T(8,128)(2,1)} %get-tuple-element.12) | copy-start | bytes 1572868

commit v2 on v1

--- a/solution.py
+++ b/solution.py
@@ -319,9 +319,9 @@
         functools.partial(kernel, n_rep),
         name="ffn_backward",
         out_shape=(
-            jax.ShapeDtypeStruct((half, width), BF16),
-            jax.ShapeDtypeStruct((width, hidden), BF16),
-            jax.ShapeDtypeStruct((hidden, width), BF16),
+            pltpu.VMEM((half, width), BF16),
+            pltpu.VMEM((width, hidden), BF16),
+            pltpu.VMEM((hidden, width), BF16),
         ),
         in_specs=[vmem, vmem, vmem, anywhere, anywhere],
         out_specs=(vmem, vmem, vmem),
@@ -348,7 +348,7 @@
             *ring, *ring, *ring, *ring,
         ],
         compiler_params=pltpu.CompilerParams(
-            collective_id=0, has_side_effects=True, vmem_limit_bytes=58 * 2**20
+            collective_id=0, has_side_effects=True, vmem_limit_bytes=48 * 2**20
         ),
     )(inputs, pre_act, cotangent, up_weight, down_weight)
     factor = (half * n_rep * lax.axis_size("tp")) ** (-0.5)

time: 193 us -> 187 us (0.969)
  Pallas kernels: 180 us -> 176 us
  other arithmetic: 11.5 us -> 9.19 us
    pallas_call x1, Pallas kernels: 180 us -> 176 us  [per_device(): pl.pallas_call(functools.partial(kernel, n_rep), name='ffn_backward', out...]
    mul x1, other arithmetic: 6.93 us -> 4.59 us  [per_device(): grad_up.astype(F32) * factor]
where the time goes in v2:
time: 187 us
  Pallas kernels  176 us (94%)
  other arithmetic  9.19 us (5%)
    pallas_call x1, Pallas kernels, per_device(): pl.pallas_call(functools.partial(kernel, n_rep), name='ffn_backward', out...  176 us
    mul x1, other arithmetic, per_device(): grad_down.astype(F32) * factor  4.6 us
    mul x1, other arithmetic, per_device(): grad_up.astype(F32) * factor  4.59 us

profile of v2, /device:TPU:0, one launch (start us, length us, event | category | flops | bytes accessed | tf_op | source)
XLA Modules:
  0.0 186.9 jit_solution(5160200714777072599)
XLA Ops:
  0.6 176.2 %ffn_backward.1 = (bf16[256,1024]{1,0:T(8,128)(2,1)S(1)}, bf16[1024,2048]{1,0:T(8,128)(2,1)S(1)}, bf16[2048,1024]{1,0:T(8,128)(2,1)S(1)}) custom-call(bf16[256,1024]{1,0:T(8,128)(2,1)} %x_ref.1, bf16[256,2048]{1,0:T(8,128)(2,1)} %pre_ref.1, bf16[256,1024]{1,0:T(8,128)(2,1)} %cot_ref.1, bf16[1024,2048]{1,0:T(8,128)(2,1)} %wu_hbm.1, bf16[2048,1024]{1,0:T(8,128)(2,1)} %wd_hbm.1), custom_call_target="tpu_custom_call" | custom-call | tf_op jit(solution)/shard_map/ffn_backward/pallas_call | solution.py:318
  176.9 0.8 copy.9
  177.7 4.6 %convert_multiply_fusion.1 = f32[1024,2048]{1,0:T(8,128)} fusion(bf16[1024,2048]{1,0:T(8,128)(2,1)S(1)} %get-tuple-element.7), kind=kLoop, calls=%fused_computation.1 | loop fusion | flops 4194304 | bytes 12582912 | tf_op jit(solution)/shard_map/mul | solution.py:355
  182.3 4.6 %convert_multiply_fusion = f32[2048,1024]{1,0:T(8,128)} fusion(bf16[2048,1024]{1,0:T(8,128)(2,1)S(1)} %get-tuple-element.8), kind=kLoop, calls=%fused_computation | loop fusion | flops 4194304 | bytes 12582912 | tf_op jit(solution)/shard_map/mul | solution.py:355

commit v3 on v2

--- a/solution.py
+++ b/solution.py
@@ -22,7 +22,8 @@
 
 def plan(n_rep, width, hidden):
     panels = hidden // LANES
-    subs = 2 if width * panels // (4 * n_rep) >= 2 * LANES else 1
+    room = width * panels // (2 * n_rep)
+    subs = max(n for n in (1, 2, 4) if n == 1 or room // n >= 2 * LANES)
     per_panel = 2 * n_rep * subs // panels
     return subs, per_panel, width // per_panel
 
@@ -241,6 +242,8 @@
         gp_copy(panel).start()
     in_order(pre_grad)
     x_move.wait_recv()
+    for d, sub in streams:
+        ag_step(down_at, agd_s, agd_r, 1, d, sub)
     if fine:
         prepare(gp_arrived, 0)
     else:
@@ -250,10 +253,13 @@
     def both_step(j, _):
         prepare(gp_arrived, j)
         for d, sub in streams:
-            ag_step(down_at, agd_s, agd_r, j, d, sub)
+            ag_step(down_at, agd_s, agd_r, j + 1, d, sub)
             rs_step(up_block, *up, j, d, sub)
         return 0
-    lax.fori_loop(1, n_rep - 1, both_step, 0)
+    lax.fori_loop(1, n_rep - 2, both_step, 0)
+    prepare(gp_arrived, n_rep - 2)
+    for d, sub in streams:
+        rs_step(up_block, *up, n_rep - 2, d, sub)
     prepare(gp_arrived, n_rep - 1)
     for d, sub in streams:
         ag_close(down_at, agd_s, agd_r, d, sub)
@@ -348,7 +354,7 @@
             *ring, *ring, *ring, *ring,
         ],
         compiler_params=pltpu.CompilerParams(
-            collective_id=0, has_side_effects=True, vmem_limit_bytes=48 * 2**20
+            collective_id=0, has_side_effects=True, vmem_limit_bytes=50 * 2**20
         ),
     )(inputs, pre_act, cotangent, up_weight, down_weight)
     factor = (half * n_rep * lax.axis_size("tp")) ** (-0.5)

time: 187 us -> 187 us (level)
  no operation moved by 1% of the time
where the time goes in v3:
time: 187 us
  Pallas kernels  176 us (94%)
  other arithmetic  9.19 us (5%)
    pallas_call x1, Pallas kernels, per_device(): pl.pallas_call(functools.partial(kernel, n_rep), name='ffn_backward', out...  176 us
    mul x1, other arithmetic, per_device(): grad_down.astype(F32) * factor  4.6 us
    mul x1, other arithmetic, per_device(): grad_up.astype(F32) * factor  4.59 us

profile of v3, /device:TPU:0, one launch (start us, length us, event | category | flops | bytes accessed | tf_op | source)
XLA Modules:
  0.0 186.8 jit_solution(17832227864547277079)
XLA Ops:
  0.6 176.2 %ffn_backward.1 = (bf16[256,1024]{1,0:T(8,128)(2,1)S(1)}, bf16[1024,2048]{1,0:T(8,128)(2,1)S(1)}, bf16[2048,1024]{1,0:T(8,128)(2,1)S(1)}) custom-call(bf16[256,1024]{1,0:T(8,128)(2,1)} %x_ref.1, bf16[256,2048]{1,0:T(8,128)(2,1)} %pre_ref.1, bf16[256,1024]{1,0:T(8,128)(2,1)} %cot_ref.1, bf16[1024,2048]{1,0:T(8,128)(2,1)} %wu_hbm.1, bf16[2048,1024]{1,0:T(8,128)(2,1)} %wd_hbm.1), custom_call_target="tpu_custom_call" | custom-call | tf_op jit(solution)/shard_map/ffn_backward/pallas_call | solution.py:324
  176.8 0.8 copy.9
  177.6 4.6 %convert_multiply_fusion.1 = f32[1024,2048]{1,0:T(8,128)} fusion(bf16[1024,2048]{1,0:T(8,128)(2,1)S(1)} %get-tuple-element.7), kind=kLoop, calls=%fused_computation.1 | loop fusion | flops 4194304 | bytes 12582912 | tf_op jit(solution)/shard_map/mul | solution.py:361
  182.2 4.6 %convert_multiply_fusion = f32[2048,1024]{1,0:T(8,128)} fusion(bf16[2048,1024]{1,0:T(8,128)(2,1)S(1)} %get-tuple-element.8), kind=kLoop, calls=%fused_computation | loop fusion | flops 4194304 | bytes 12582912 | tf_op jit(solution)/shard_map/mul | solution.py:361

commit v4 on v3

--- a/solution.py
+++ b/solution.py
@@ -29,9 +29,9 @@
 
 
 def kernel(
-    n_rep, x_ref, pre_ref, cot_ref, wu_hbm, wd_hbm,
+    n_rep, x_hbm, pre_hbm, cot_hbm, wu_hbm, wd_hbm,
     gi_ref, up_ref, down_ref,
-    wu, wd, xg, cg, pre_in, sq, gp, pa_own, pa_out, pa_in, gi_out, gi_in,
+    x_ref, pre_ref, cot_ref, wu, wd, xg, cg, pre_in, sq, gp, pa_own, pa_out, pa_in, gi_out, gi_in,
     first_d, first_u, rs_d, rs_u,
     w_sem, tp_s, tp_r, pre_s, pre_r, gp_s, gp_r, pa_s, pa_r, gi_s, gi_r,
     rsd_s, rsd_r, rsu_s, rsu_r, agd_s, agd_r, agu_s, agu_r,
@@ -63,14 +63,16 @@
             src_ref=src, dst_ref=dst, send_sem=s, recv_sem=r, device_id=dev,
             device_id_type=MESH)
 
-    load_wd = pltpu.make_async_copy(wd_hbm, wd, w_sem.at[0])
-    load_wu = pltpu.make_async_copy(wu_hbm, wu, w_sem.at[1])
-    load_wd.start()
-    load_wu.start()
-
     barrier = pltpu.get_barrier_semaphore()
     for dev in (goal[0], goal[1], other_fs, other_tp):
         pl.semaphore_signal(barrier, inc=1, device_id=dev, device_id_type=MESH)
+    held = ((cot_hbm, cot_ref), (pre_hbm, pre_ref), (x_hbm, x_ref), (wd_hbm, wd), (wu_hbm, wu))
+    loads = [pltpu.make_async_copy(src, dst, w_sem.at[i]) for i, (src, dst) in enumerate(held)]
+    load_cot, load_pre, load_x, load_wd, load_wu = loads
+    for load in loads:
+        load.start()
+    load_cot.wait()
+    load_pre.wait()
     pl.semaphore_wait(barrier, 4)
 
     def chunk_of(d, j):
@@ -107,6 +109,7 @@
     x_move = remote(x_ref, xg.at[mine_t, :], tp_s.at[1], tp_r.at[1], other_tp)
     cot_move.start()
     in_order(lambda panel: pre_copy(panel).start())
+    load_x.wait()
     x_move.start()
     cg[mine_t, :] = cot_ref[...]
     xg[mine_t, :] = x_ref[...]
@@ -310,6 +313,21 @@
             ag_copy(up_at, agu_s, agu_r, d, sub, s).wait_send()
         return 0
     lax.fori_loop(0, n_rep - 1, sent_steps, 0)
+
+
+def scale_kernel(factor, pieces, gi, up, down, gi_out, up_out, down_out, up_wide, down_wide,
+                 sems, gi_sem):
+    copies = [pltpu.make_async_copy(gi, gi_out, gi_sem)]
+    copies[0].start()
+    for i in range(pieces):
+        for n, (src, wide, dst) in enumerate(((up, up_wide, up_out), (down, down_wide, down_out))):
+            rows = pl.ds(i * (src.shape[0] // pieces), src.shape[0] // pieces)
+            wide[rows, :] = src[rows, :].astype(F32) * factor
+            copy = pltpu.make_async_copy(wide.at[rows, :], dst.at[rows, :], sems.at[n, i])
+            copy.start()
+            copies.append(copy)
+    for copy in copies:
+        copy.wait()
 
 
 def per_device(n_rep, inputs, pre_act, cotangent, up_weight, down_weight):
@@ -329,9 +347,12 @@
             pltpu.VMEM((width, hidden), BF16),
             pltpu.VMEM((hidden, width), BF16),
         ),
-        in_specs=[vmem, vmem, vmem, anywhere, anywhere],
+        in_specs=[anywhere] * 5,
         out_specs=(vmem, vmem, vmem),
         scratch_shapes=[
+            pltpu.VMEM((half, width), BF16),
+            pltpu.VMEM((half, hidden), BF16),
+            pltpu.VMEM((half, width), BF16),
             pltpu.VMEM((width, hidden), BF16),
             pltpu.VMEM((hidden, width), BF16),
             pltpu.VMEM((2 * half, width), BF16),
@@ -348,7 +369,7 @@
             pltpu.VMEM((2, subs, w, LANES), BF16),
             pltpu.VMEM((2, subs, n_rep - 1, LANES, w), BF16),
             pltpu.VMEM((2, subs, n_rep - 1, w, LANES), BF16),
-            dma((2,)), dma((2,)), dma((2,)),
+            dma((5,)), dma((2,)), dma((2,)),
             dma((panels,)), dma((panels,)), dma((panels,)), dma((panels,)),
             dma, dma, dma, dma,
             *ring, *ring, *ring, *ring,
@@ -358,7 +379,26 @@
         ),
     )(inputs, pre_act, cotangent, up_weight, down_weight)
     factor = (half * n_rep * lax.axis_size("tp")) ** (-0.5)
-    return grad_inputs, grad_up.astype(F32) * factor, grad_down.astype(F32) * factor
+    pieces = 8
+    return pl.pallas_call(
+        functools.partial(scale_kernel, factor, pieces),
+        name="scale_outputs",
+        out_shape=(
+            jax.ShapeDtypeStruct((half, width), BF16),
+            jax.ShapeDtypeStruct((width, hidden), F32),
+            jax.ShapeDtypeStruct((hidden, width), F32),
+        ),
+        in_specs=[vmem] * 3,
+        out_specs=[anywhere] * 3,
+        scratch_shapes=[
+            pltpu.VMEM((width, hidden), F32),
+            pltpu.VMEM((hidden, width), F32),
+            dma((2, pieces)),
+            dma,
+        ],
+        compiler_params=pltpu.CompilerParams(vmem_limit_bytes=40 * 2**20),
+    )(*[pltpu.with_memory_space_constraint(g, pltpu.VMEM)
+        for g in (grad_inputs, grad_up, grad_down)])
 
 
 def solution(mesh):

time: 187 us -> 182 us (0.973)
  other arithmetic: 9.19 us -> 0 us
  Pallas kernels: 176 us -> 181 us
    mul x2 -> x0, other arithmetic: 9.19 us -> none  [the longest x1 4.6 us: per_device(): grad_down.astype(F32) * factor]
    pallas_call x0 -> x1, Pallas kernels: none -> 6.2 us  [per_device(): pl.pallas_call(functools.partial(scale_kernel, factor, pieces), name='sca...]
where the time goes in v4:
time: 182 us
  Pallas kernels  181 us (99%)
    pallas_call x1, Pallas kernels, per_device(): pl.pallas_call(functools.partial(kernel, n_rep), name='ffn_backward', out...  175 us
    pallas_call x1, Pallas kernels, per_device(): pl.pallas_call(functools.partial(scale_kernel, factor, pieces), name='sca...  6.2 us

profile of v4, /device:TPU:0, one launch (start us, length us, event | category | flops | bytes accessed | tf_op | source)
XLA Modules:
  0.0 181.7 jit_solution(9845751893619549068)
XLA Ops:
  0.6 174.7 %ffn_backward.1 = (bf16[256,1024]{1,0:T(8,128)(2,1)S(1)}, bf16[1024,2048]{1,0:T(8,128)(2,1)S(1)}, bf16[2048,1024]{1,0:T(8,128)(2,1)S(1)}) custom-call(bf16[256,1024]{1,0:T(8,128)(2,1)} %x_hbm.1, bf16[256,2048]{1,0:T(8,128)(2,1)} %pre_hbm.1, bf16[256,1024]{1,0:T(8,128)(2,1)} %cot_hbm.1, bf16[1024,2048]{1,0:T(8,128)(2,1)} %wu_hbm.1, bf16[2048,1024]{1,0:T(8,128)(2,1)} %wd_hbm.1), custom_call_target="tpu_custom_call" | custom-call | tf_op jit(solution)/shard_map/ffn_backward/pallas_call | solution.py:342
  175.4 6.2 %scale_outputs.1 = (bf16[256,1024]{1,0:T(8,128)(2,1)}, f32[1024,2048]{1,0:T(8,128)}, f32[2048,1024]{1,0:T(8,128)}) custom-call(bf16[256,1024]{1,0:T(8,128)(2,1)S(1)} %get-tuple-element.6.gi, bf16[1024,2048]{1,0:T(8,128)(2,1)S(1)} %get-tuple-element.7.up, bf16[2048,1024]{1,0:T(8,128)(2,1)S(1)} %get-tuple-element.8.down), custom_call_target="tpu_custom_call" | custom-call | tf_op jit(solution)/shard_map/scale_outputs/pallas_call | solution.py:383

commit v5 on v4

--- a/solution.py
+++ b/solution.py
@@ -23,7 +23,7 @@
 def plan(n_rep, width, hidden):
     panels = hidden // LANES
     room = width * panels // (2 * n_rep)
-    subs = max(n for n in (1, 2, 4) if n == 1 or room // n >= 2 * LANES)
+    subs = max(n for n in (1, 2) if n == 1 or room // n >= 2 * LANES)
     per_panel = 2 * n_rep * subs // panels
     return subs, per_panel, width // per_panel
 

time: 182 us -> 180 us (0.989)
  Pallas kernels: 181 us -> 179 us
where the time goes in v5:
time: 180 us
  Pallas kernels  179 us (99%)
    pallas_call x1, Pallas kernels, per_device(): pl.pallas_call(functools.partial(kernel, n_rep), name='ffn_backward', out...  173 us
    pallas_call x1, Pallas kernels, per_device(): pl.pallas_call(functools.partial(scale_kernel, factor, pieces), name='sca...  6.2 us

profile of v5, /device:TPU:0, one launch (start us, length us, event | category | flops | bytes accessed | tf_op | source)
XLA Modules:
  0.0 179.8 jit_solution(15156822450796210993)
XLA Ops:
  0.6 172.9 %ffn_backward.1 = (bf16[256,1024]{1,0:T(8,128)(2,1)S(1)}, bf16[1024,2048]{1,0:T(8,128)(2,1)S(1)}, bf16[2048,1024]{1,0:T(8,128)(2,1)S(1)}) custom-call(bf16[256,1024]{1,0:T(8,128)(2,1)} %x_hbm.1, bf16[256,2048]{1,0:T(8,128)(2,1)} %pre_hbm.1, bf16[256,1024]{1,0:T(8,128)(2,1)} %cot_hbm.1, bf16[1024,2048]{1,0:T(8,128)(2,1)} %wu_hbm.1, bf16[2048,1024]{1,0:T(8,128)(2,1)} %wd_hbm.1), custom_call_target="tpu_custom_call" | custom-call | tf_op jit(solution)/shard_map/ffn_backward/pallas_call | solution.py:342
  173.6 6.2 %scale_outputs.1 = (bf16[256,1024]{1,0:T(8,128)(2,1)}, f32[1024,2048]{1,0:T(8,128)}, f32[2048,1024]{1,0:T(8,128)}) custom-call(bf16[256,1024]{1,0:T(8,128)(2,1)S(1)} %get-tuple-element.6.gi, bf16[1024,2048]{1,0:T(8,128)(2,1)S(1)} %get-tuple-element.7.up, bf16[2048,1024]{1,0:T(8,128)(2,1)S(1)} %get-tuple-element.8.down), custom_call_target="tpu_custom_call" | custom-call | tf_op jit(solution)/shard_map/scale_outputs/pallas_call | solution.py:383
